TPU v7x, 32 devices: a whole 2x2x4 slice. The times are simulated.
32 devices in a mesh: sp: 4 (over z), fs: 4 (over y, core), tp: 2 (over x).
Axes of the slice: x: 2, y: 2, z: 4, core: 2. Of those that a mesh axis runs over, the one named last changes fastest.
Arguments:
- tokens: bfloat16 [8, 2048, 2048], P('fs', ('sp', 'tp')), may hold values from -6 to 6
- norm_gain: float32 [2048], replicated, may hold values from 0.1 to 1.9
- w_pool_in: bfloat16 [2048, 1024], P('fs', 'tp'), may hold values from -0.125 to 0.125
- pool_mix: bfloat16 [8, 128, 128], replicated, may hold values from -0.5 to 0.5
- pool_scale: float32 [1024], replicated, may hold values from 0.1 to 1.9
- w_query: bfloat16 [2048, 1024], P('fs', 'tp'), may hold values from -0.13258252 to 0.13258252
- w_key: bfloat16 [2048, 1024], P('fs', 'tp'), may hold values from -0.508233 to 0.508233
- w_value: bfloat16 [2048, 1024], P('fs', 'tp'), may hold values from -0.125 to 0.125
- gate_cache: float32 [8, 8, 2048], P('fs', 'tp'), may hold values from -258 to 0, as said below
- w_out_pool: bfloat16 [1024, 2048], P('tp', 'fs'), may hold values from -0.125 to 0.125
- w_out_attn: bfloat16 [1024, 2048], P('tp', 'fs'), may hold values from -0.75 to 0.75
Outputs:
- mixed: bfloat16 [8, 2048, 2048], P('fs', ('sp', 'tp'))
Inputs may be any that keep to these rules, and one draw needn't show every extreme that they name: `gate_cache`: each head's values never rise along the positions.
All inputs are finite; a program needn't handle non-finite values.
Results may differ from a plain program's by a relative error of at most 0.014.
Values may be sent and summed in bfloat16 or wider, within the bound.
A program may use at most 128 MiB of HBM per device.

v0:
```python
import jax
import jax.numpy as jnp
from jax import lax
from jax.sharding import PartitionSpec as P

HEAD_DIM = 128
GROUP_WIDTH = 128
norm_eps = 1e-06
widest = 16
masked_score = -1e30


def shifted(x, axis, by):
    length = lax.axis_size(axis)
    pairs = [(i, i + by) for i in range(length) if 0 <= i + by < length]
    return lax.ppermute(x, axis, pairs)


def window_sums(extended):
    outcome = []
    current = extended
    offset = 1
    for doubling in range(4):
        padding = jnp.zeros((offset, extended.shape[1]), jnp.float32)
        current = current + jnp.concatenate([padding, current[:-offset]], axis=0)
        offset = offset * 2
        outcome.append(current[widest - 1 :])
    return outcome


def pool_branch(projected, border, first_group, first_position, mixing, scaling):
    row_count = projected.shape[0]
    channels = projected.shape[1]
    widened = projected.astype(jnp.float32)
    totals = window_sums(jnp.concatenate([border.astype(jnp.float32), widened], axis=0))
    token_positions = first_position + jnp.arange(row_count)
    window_index = (first_group + jnp.arange(channels) // GROUP_WIDTH) % 4
    averaged = jnp.zeros((row_count, channels), jnp.float32)
    for doubling in range(4):
        counted = jnp.minimum(token_positions + 1, 2 ** (doubling + 1)).astype(jnp.float32)
        picked = (window_index == doubling).astype(jnp.float32)
        averaged = averaged + picked[None, :] * totals[doubling] / counted[:, None]
    departure = (averaged - widened).astype(jnp.bfloat16)
    group_count = channels // GROUP_WIDTH
    mixed_rows = jnp.einsum(
        "tgc,gcd->tgd",
        departure.reshape(row_count, group_count, GROUP_WIDTH),
        mixing,
        preferred_element_type=jnp.float32,
    )
    return (mixed_rows.reshape(row_count, channels) * scaling[None, :]).astype(jnp.bfloat16)


def on_device(
    tokens,
    norm_gain,
    w_pool_in,
    pool_mix,
    pool_scale,
    w_query,
    w_key,
    w_value,
    gate_cache,
    w_out_pool,
    w_out_attn,
):
    tp_index = lax.axis_index("tp")
    tp_count = lax.axis_size("tp")
    seq_count = tokens.shape[0]
    own_count = tokens.shape[1]
    token_count = own_count * tp_count
    first_position = lax.axis_index("sp") * token_count
    own_rows = tokens.astype(jnp.float32)
    normed = (
        own_rows
        * lax.rsqrt(jnp.mean(own_rows * own_rows, axis=-1, keepdims=True) + norm_eps)
        * norm_gain[None, None, :]
    ).astype(jnp.bfloat16)
    pool_full, query_full, key_full, value_full, out_pool_full, out_attn_full = (
        lax.all_gather(w_pool_in, "fs", axis=0, tiled=True),
        lax.all_gather(w_query, "fs", axis=0, tiled=True),
        lax.all_gather(w_key, "fs", axis=0, tiled=True),
        lax.all_gather(w_value, "fs", axis=0, tiled=True),
        lax.all_gather(w_out_pool, "fs", axis=1, tiled=True),
        lax.all_gather(w_out_attn, "fs", axis=1, tiled=True),
    )
    pool_cols = w_pool_in.shape[1]
    attn_cols = w_query.shape[1]
    shard_rows = lax.all_gather(normed, "tp", axis=1, tiled=True)
    projected = jnp.concatenate(
        [
            jnp.dot(shard_rows, pool_full, preferred_element_type=jnp.float32).astype(jnp.bfloat16),
            jnp.dot(shard_rows, query_full, preferred_element_type=jnp.float32).astype(
                jnp.bfloat16
            ),
            jnp.dot(shard_rows, key_full, preferred_element_type=jnp.float32).astype(jnp.bfloat16),
            jnp.dot(shard_rows, value_full, preferred_element_type=jnp.float32).astype(
                jnp.bfloat16
            ),
        ],
        axis=2,
    )
    pool_in = projected[:, :, :pool_cols]
    query_proj = projected[:, :, pool_cols : pool_cols + attn_cols]
    key_proj = projected[:, :, pool_cols + attn_cols : pool_cols + 2 * attn_cols]
    value_proj = projected[:, :, pool_cols + 2 * attn_cols :]
    group_local = pool_cols // GROUP_WIDTH
    mixing = lax.dynamic_slice_in_dim(pool_mix, tp_index * group_local, group_local, 0)
    scaling = lax.dynamic_slice_in_dim(pool_scale, tp_index * pool_cols, pool_cols, 0)
    borders = shifted(pool_in[:, token_count - (widest - 1) :], "sp", 1)
    pool_out = jnp.stack(
        [
            pool_branch(
                pool_in[member],
                borders[member],
                tp_index * group_local,
                first_position,
                mixing,
                scaling,
            )
            for member in range(seq_count)
        ],
        axis=0,
    )
    head_count = attn_cols // HEAD_DIM
    query_heads = query_proj.reshape(seq_count, token_count, head_count, HEAD_DIM)
    query_gates = jnp.transpose(
        lax.dynamic_slice_in_dim(gate_cache, first_position, token_count, 2), (0, 2, 1)
    )
    query_positions = first_position + jnp.arange(token_count)
    last_position = first_position + token_count - 1
    score_scale = HEAD_DIM ** (-0.5)
    start_state = (
        jnp.full((seq_count, token_count, head_count), masked_score, jnp.float32),
        jnp.zeros((seq_count, token_count, head_count), jnp.float32),
        jnp.zeros((seq_count, token_count, head_count, HEAD_DIM), jnp.float32),
    )
    key_shard = lax.all_gather(key_proj, "sp", axis=1, tiled=True)
    value_shard = lax.all_gather(value_proj, "sp", axis=1, tiled=True)
    key_total = key_shard.shape[1]
    block_rows = 512

    def one_block(block_state, block_index):
        key_start = block_index * block_rows

        def compute(inner_state):
            running_top, running_sum, running_out = inner_state
            key_block = lax.dynamic_slice_in_dim(key_shard, block_index * block_rows, block_rows, 1)
            value_block = lax.dynamic_slice_in_dim(
                value_shard, block_index * block_rows, block_rows, 1
            )
            key_block = key_block.reshape(seq_count, block_rows, head_count, HEAD_DIM)
            value_block = value_block.reshape(seq_count, block_rows, head_count, HEAD_DIM)
            key_gates = lax.dynamic_slice_in_dim(gate_cache, key_start, block_rows, 2)
            scores = (
                jnp.einsum(
                    "sqhd,skhd->sqhk", query_heads, key_block, preferred_element_type=jnp.float32
                )
                * score_scale
            )
            scores = scores + query_gates[:, :, :, None] - key_gates[:, None, :, :]
            allowed = ((key_start + jnp.arange(block_rows))[None, :] <= query_positions[:, None])[
                None, :, None, :
            ]
            scores = jnp.where(allowed, scores, masked_score)
            new_top = jnp.maximum(running_top, jnp.max(scores, axis=3))
            weights = jnp.where(allowed, jnp.exp(scores - new_top[:, :, :, None]), 0.0)
            shrink = jnp.exp(running_top - new_top)
            running_sum = running_sum * shrink + jnp.sum(weights, axis=3)
            running_out = running_out * shrink[:, :, :, None] + jnp.einsum(
                "sqhk,skhd->sqhd",
                weights.astype(jnp.bfloat16),
                value_block,
                preferred_element_type=jnp.float32,
            )
            return (new_top, running_sum, running_out)

        def unchanged(inner_state):
            return inner_state

        return (lax.cond(key_start <= last_position, compute, unchanged, block_state), None)

    result, unused = lax.scan(one_block, start_state, jnp.arange(key_total // block_rows))
    final_top, final_sum, final_out = result
    attn_out = (
        (final_out / final_sum[:, :, :, None])
        .astype(jnp.bfloat16)
        .reshape(seq_count, token_count, attn_cols)
    )
    pool_flat = jnp.transpose(
        pool_out.reshape(seq_count, tp_count, own_count, pool_cols), (1, 0, 2, 3)
    ).reshape(tp_count * seq_count * own_count, pool_cols)
    attn_flat = jnp.transpose(
        attn_out.reshape(seq_count, tp_count, own_count, attn_cols), (1, 0, 2, 3)
    ).reshape(tp_count * seq_count * own_count, attn_cols)
    summed = lax.psum_scatter(
        (
            jnp.dot(pool_flat, out_pool_full, preferred_element_type=jnp.float32)
            + jnp.dot(attn_flat, out_attn_full, preferred_element_type=jnp.float32)
        ).astype(jnp.bfloat16),
        "tp",
        scatter_dimension=0,
        tiled=True,
    ).astype(jnp.float32)
    return summed.astype(jnp.bfloat16).reshape(seq_count, own_count, summed.shape[1])


def solution(mesh):
    placed = (
        P("fs", ("sp", "tp"), None),
        P(),
        P("fs", "tp"),
        P(),
        P(),
        P("fs", "tp"),
        P("fs", "tp"),
        P("fs", "tp"),
        P("fs", "tp", None),
        P("tp", "fs"),
        P("tp", "fs"),
    )
    return jax.shard_map(
        on_device,
        mesh=mesh,
        in_specs=placed,
        out_specs=P("fs", ("sp", "tp"), None),
        check_vma=False,
    )
```

profile of v0, /device:TPU:0, one launch (start us, length us, event | category | flops | bytes accessed | tf_op | source)
XLA Modules:
  0.0 483.2 jit_solution(8892311270368384525)
XLA Ops:
  14.4 19.8 %all-gather.16.cloned.1.call-done = bf16[2048,512]{1,0:T(8,128)(2,1)} async-done(((bf16[512,512]{1,0:T(8,128)(2,1)}), bf16[2048,512]{1,0:T(8,128)(2,1)}) %all-gather.16.cloned.1.call-update) | async-done | bytes 2097168 | tf_op jit(solution)/shard_map/all_gather | solution.py:82
  34.2 58.3 %all-gather.10.cloned.1.call-done = bf16[2,512,2048]{2,1,0:T(8,128)(2,1)} async-done(((bf16[2,256,2048]{2,1,0:T(8,128)(2,1)}), bf16[2,512,2048]{2,1,0:T(8,128)(2,1)}) %all-gather.10.cloned.1.call-update) | async-done | bytes 4194320 | tf_op jit(solution)/shard_map/all_gather | solution.py:89
  92.5 6.2 %fusion.29 = bf16[2,512,512]{2,1,0:T(8,128)(2,1)} fusion(bf16[2,512,2048]{2,1,0:T(8,128)(2,1)} %all-gather.10.cloned.1.call-done, bf16[2048,512]{1,0:T(8,128)(2,1)} %all-gather.16.cloned.1.call-done), kind=kOutput, calls=%fused_computation.42 | convolution fusion | flops 2148007936 | bytes 7340032 | tf_op jit(solution)/shard_map/dot_general | solution.py:96
  98.8 17.9 %all-gather.22.cloned.1.call-done = bf16[2048,512]{1,0:T(8,128)(2,1)} async-done(((bf16[512,512]{1,0:T(8,128)(2,1)}), bf16[2048,512]{1,0:T(8,128)(2,1)}) %all-gather.22.cloned.1.call-update) | async-done | bytes 2097168 | tf_op jit(solution)/shard_map/all_gather | solution.py:83
  116.7 6.2 %fusion.35 = bf16[2,512,512]{2,1,0:T(8,128)(2,1)} fusion(bf16[2,512,2048]{2,1,0:T(8,128)(2,1)} %all-gather.10.cloned.1.call-done, bf16[2048,512]{1,0:T(8,128)(2,1)} %all-gather.22.cloned.1.call-done), kind=kOutput, calls=%fused_computation.44 | convolution fusion | flops 2148007936 | bytes 7340032 | tf_op jit(solution)/shard_map/dot_general | solution.py:97
  124.4 16.3 %all-gather.12.cloned.1.call-done = bf16[2048,512]{1,0:T(8,128)(2,1)} async-done(((bf16[512,512]{1,0:T(8,128)(2,1)}), bf16[2048,512]{1,0:T(8,128)(2,1)}) %all-gather.12.cloned.1.call-update) | async-done | bytes 2097168 | tf_op jit(solution)/shard_map/all_gather | solution.py:80
  140.7 5.2 %fusion.26 = bf16[2,512,512]{2,1,0:T(8,128)(2,1)S(1)} fusion(bf16[2,512,2048]{2,1,0:T(8,128)(2,1)} %all-gather.10.cloned.1.call-done, bf16[2048,512]{1,0:T(8,128)(2,1)} %all-gather.12.cloned.1.call-done), kind=kOutput, calls=%fused_computation.41 | convolution fusion | flops 2148007936 | bytes 7340032 | tf_op jit(solution)/shard_map/dot_general | solution.py:92
  145.9 4.0 collective-permute-start
  149.9 14.8 %all-gather.20.cloned.1.call-done = bf16[2048,512]{0,1:T(8,128)(2,1)} async-done(((bf16[512,512]{0,1:T(8,128)(2,1)}), bf16[2048,512]{0,1:T(8,128)(2,1)}) %all-gather.20.cloned.1.call-update) | async-done | bytes 2097168 | tf_op jit(solution)/shard_map/all_gather | solution.py:81
  164.7 6.2 %fusion.32 = bf16[2,512,512]{1,2,0:T(8,128)(2,1)} fusion(bf16[2,512,2048]{2,1,0:T(8,128)(2,1)} %all-gather.10.cloned.1.call-done, bf16[2048,512]{0,1:T(8,128)(2,1)} %all-gather.20.cloned.1.call-done), kind=kOutput, calls=%fused_computation.43 | convolution fusion | flops 2148007936 | bytes 7340032 | tf_op jit(solution)/shard_map/dot_general | solution.py:93
  176.3 2.9 fusion.67
  184.4 4.3 all-gather.14.cloned.1.call-done
  188.7 7.2 %fusion.79 = f32[1024,2048]{1,0:T(8,128)} fusion(bf16[1024,512]{1,0:T(8,128)(2,1)S(1)} %bitcast.129, bf16[512,2048]{1,0:T(8,128)(2,1)} %all-gather.14.cloned.1.call-done), kind=kOutput, calls=%fused_computation.123 | convolution fusion | flops 2147483648 | bytes 11534336 | tf_op jit(solution)/shard_map/dot_general | solution.py:198
  195.9 75.1 %all-gather.18.cloned.1.call-done = bf16[2,2048,512]{2,1,0:T(8,128)(2,1)} async-done(((bf16[2,512,512]{2,1,0:T(8,128)(2,1)}), bf16[2,2048,512]{2,1,0:T(8,128)(2,1)}) %all-gather.18.cloned.1.call-update) | async-done | bytes 4194320 | tf_op jit(solution)/shard_map/all_gather | solution.py:138
  271.0 6.3 %copy.38 = bf16[2,2048,512]{1,2,0:T(8,128)(2,1)} copy(bf16[2,2048,512]{2,1,0:T(8,128)(2,1)} %all-gather.18.cloned.1.call-done) | data formatting | bytes 8388608
  277.3 74.5 %all-gather.24.cloned.1.call-done = bf16[2,2048,512]{2,1,0:T(8,128)(2,1)} async-done(((bf16[2,512,512]{2,1,0:T(8,128)(2,1)}), bf16[2,2048,512]{2,1,0:T(8,128)(2,1)}) %all-gather.24.cloned.1.call-update) | async-done | bytes 4194320 | tf_op jit(solution)/shard_map/all_gather | solution.py:139
  351.9 6.3 %copy.40 = bf16[2,2048,512]{1,2,0:T(8,128)(2,1)} copy(bf16[2,2048,512]{2,1,0:T(8,128)(2,1)} %all-gather.24.cloned.1.call-done) | data formatting | bytes 8388608
  359.5 17.2 %while.15 = (s32[]{:T(128)}, f32[2,512,4]{1,2,0:T(4,128)S(1)}, f32[2,512,4]{1,2,0:T(4,128)S(1)}, f32[2,512,4,128]{1,3,2,0:T(8,128)S(1)}, s32[4]{0:T(128)S(1)}, /...) while((s32[]{:T(128)}, f32[2,512,4]{1,2,0:T(4,128)S(1)}, ...), condition=%wide.region_6.7_spmd.clone, body=%wide.region_1.6_spmd.clone.sunk | while | flops 1114907648 | bytes 38154664 | solution.py:183
  360.7 12.1 %conditional.3 = ((f32[2,512,4]{1,2,0:T(4,128)S(1)}, f32[2,512,4]{1,2,0:T(4,128)S(1)}, f32[2,512,4,128]{1,3,2,0:T(8,128)S(1)})) conditional(s32[]{:T(128)} %convert_element_type.217, (f32[2,512,4]{1,2,0:T(4,128)S(1)}, f32[2,512,4]{1,2,0:T(4,128)S(1)}, f32[2,512,4,128]{1,3,2,0:T(8,128)S(1)}) %tuple.49, (s32[]{:T(128)}, s32[]{:T(128)}, s32[]{:T(128)}, ...), branch_computations={%region_2.2_spmd, %region_3.5_spmd} | conditional | flops 1114907648 | bytes 38152320 | solution.py:181
  363.4 2.6 fusion.6
  366.0 3.2 fusion.5
  369.2 3.5 bitcast_add_fusion.1
  378.8 8.4 %add_convert_fusion = bf16[1024,2048]{1,0:T(8,128)(2,1)} fusion(f32[1024,2048]{1,0:T(8,128)} %fusion.79, bf16[1024,512]{1,0:T(8,128)(2,1)S(1)} %bitcast.130, bf16[512,2048]{1,0:T(8,128)(2,1)} %all-gather.26.cloned.1.call-done), kind=kOutput, calls=%fused_computation.22 | convolution fusion | flops 2151677952 | bytes 15728640 | tf_op jit(solution)/shard_map/dot_general | solution.py:199
  387.2 89.2 %reduce-scatter.2.cloned.1.call-done = bf16[512,2048]{1,0:T(8,128)(2,1)} async-done(((bf16[1024,2048]{1,0:T(8,128)(2,1)}), bf16[512,2048]{1,0:T(8,128)(2,1)}) %reduce-scatter.2.cloned.1.call-update) | async-done | bytes 2097168 | tf_op jit(solution)/shard_map/reduce_scatter | solution.py:196
  (96 shorter events, 27.4 us)
Async XLA Ops:
  6.5 172.7 %copy-start = (bf16[8,128,128]{2,1,0:T(8,128)(2,1)S(1)}, bf16[8,128,128]{2,1,0:T(8,128)(2,1)}, u32[]{:S(2)}) copy-start(bf16[8,128,128]{2,1,0:T(8,128)(2,1)} %param.18) | copy-start | bytes 786436
  6.5 2.9 copy-start.2
  6.5 2.9 copy-start.6
  6.5 27.7 %all-gather.16.cloned.1.call-start = ((), (), s32[]{:S(2)}) async-start(), calls=%async_computation.4 | async-start | bytes 2621440 | tf_op jit(solution)/shard_map/all_gather | solution.py:82
  7.3 85.2 %all-gather.10.cloned.1.call-start = ((), (), s32[]{:S(2)}) async-start(), calls=%async_computation.1 | async-start | bytes 6291456 | tf_op jit(solution)/shard_map/all_gather | solution.py:89
  11.3 1.4 copy-start.4
  11.3 105.4 %all-gather.22.cloned.1.call-start = ((), (), s32[]{:S(2)}) async-start(), calls=%async_computation.7 | async-start | bytes 2621440 | tf_op jit(solution)/shard_map/all_gather | solution.py:83
  12.0 128.6 %all-gather.12.cloned.1.call-start = ((), (), s32[]{:S(2)}) async-start(), calls=%async_computation.2 | async-start | bytes 2621440 | tf_op jit(solution)/shard_map/all_gather | solution.py:80
  12.6 152.1 %all-gather.20.cloned.1.call-start = ((), (), s32[]{:S(2)}) async-start(), calls=%async_computation.6 | async-start | bytes 2621440 | tf_op jit(solution)/shard_map/all_gather | solution.py:81
  13.7 175.0 %all-gather.14.cloned.1.call-start = ((), (), s32[]{:S(2)}) async-start(), calls=%async_computation.3 | async-start | bytes 2621440 | tf_op jit(solution)/shard_map/all_gather | solution.py:84
  14.3 256.7 %all-gather.18.cloned.1.call-start = ((), (), s32[]{:S(2)}) async-start(), calls=%async_computation.5 | async-start | bytes 5242880 | tf_op jit(solution)/shard_map/all_gather | solution.py:138
  98.7 25.0 %copy-start.8 = (f32[1024]{0:T(1024)S(1)}, f32[1024]{0:T(1024)}, u32[]{:S(2)}) copy-start(f32[1024]{0:T(1024)} %param.19) | copy-start | bytes 12292
  98.7 25.7 %copy-start.5 = (f32[2,4,2048]{2,1,0:T(4,128)S(1)}, f32[2,4,2048]{2,1,0:T(4,128)}, u32[]{:S(2)}) copy-start(f32[2,4,2048]{2,1,0:T(4,128)} %param.23) | copy-start | bytes 196612
  98.7 253.1 %all-gather.24.cloned.1.call-start = ((), (), s32[]{:S(2)}) async-start(), calls=%async_computation.8 | async-start | bytes 5242880 | tf_op jit(solution)/shard_map/all_gather | solution.py:139
  122.9 255.9 %all-gather.26.cloned.1.call-start = ((), (), s32[]{:S(2)}) async-start(), calls=%async_computation.9 | async-start | bytes 2621440 | tf_op jit(solution)/shard_map/all_gather | solution.py:85
  123.6 352.8 %reduce-scatter.2.cloned.1.call-start = ((), (), s32[]{:S(2)}) async-start(), calls=%async_computation.10 | async-start | bytes 6291456 | tf_op jit(solution)/shard_map/reduce_scatter | solution.py:196
  145.9 27.6 %collective-permute-start = (bf16[2,15,512]{2,1,0:T(8,128)(2,1)S(1)}, bf16[2,15,512]{2,1,0:T(8,128)(2,1)}, u32[]{:S(2)}, u32[]{:S(2)}) collective-permute-start(bf16[2,15,512]{2,1,0:T(8,128)(2,1)S(1)} %slice.84), channel_id=1, source_target_pairs={{0,8},{8,16},{16,24},{1,9},{9,17},{17,25},{2,10},{10,18},{18,26},{... | collective-permute-start | bytes 92168 | tf_op jit(solution)/shard_map/ppermute | solution.py:16
  182.5 1.5 copy-start.7
  358.2 1.3 copy-start.3
  387.2 89.2 %copy-start.1 = (bf16[8,128,128]{2,1,0:T(8,128)(2,1)S(1)}, bf16[8,128,128]{2,1,0:T(8,128)(2,1)}, u32[]{:S(2)}) copy-start(bf16[8,128,128]{2,1,0:T(8,128)(2,1)} %param.18) | copy-start | bytes 786436
Sparse Core Ops, SparseCore 0:
  8.9 25.2 all-gather.15
  35.8 56.7 all-gather.9
  94.1 22.5 all-gather.21
  118.1 22.5 all-gather.11
  142.1 22.5 all-gather.19
  166.1 22.5 all-gather.13
  190.3 80.7 all-gather.17
  272.6 79.2 all-gather.23
  353.4 21.0 all-gather.25
  387.3 89.0 reduce-scatter.1
where the time goes:
time: 484 us; the launch traced here: 483 us
  waiting for transfers between devices  374 us (77%)
  matrix products  47.3 us (10%)
  local copies, waits for them, and re-layouts  27 us (6%)
  other arithmetic  13.8 us (3%)
  between operations  13.8 us (3%)
    reduce_scatter x1, waiting for transfers between devices, on_device(): lax.psum_scatter((jnp.dot(pool_flat, out_pool_full, preferred_element_typ...  89.2 us
    all_gather x1, waiting for transfers between devices, on_device(): key_shard = lax.all_gather(key_proj, 'sp', axis=1, tiled=True)  75.1 us
    all_gather x1, waiting for transfers between devices, on_device(): value_shard = lax.all_gather(value_proj, 'sp', axis=1, tiled=True)  74.5 us
    all_gather x1, waiting for transfers between devices, on_device(): shard_rows = lax.all_gather(normed, 'tp', axis=1, tiled=True)  58.3 us
    all_gather x1, waiting for transfers between devices, on_device(): lax.all_gather(w_key, 'fs', axis=0, tiled=True)  19.8 us
    all_gather x1, waiting for transfers between devices, on_device(): lax.all_gather(w_value, 'fs', axis=0, tiled=True)  17.9 us
    unnamed x22, local copies, waits for them, and re-layouts  17 us
    all_gather x1, waiting for transfers between devices, on_device(): lax.all_gather(w_pool_in, 'fs', axis=0, tiled=True)  16.3 us
  transfers between devices with their start and end apart: 11, of which 9 were waited for; matrix products, arithmetic and copies ran while one was open for 16% of the time, Pallas kernels for 0%

commit v1 on v0

--- a/solution.py
+++ b/solution.py
@@ -135,7 +135,12 @@
         jnp.zeros((seq_count, token_count, head_count), jnp.float32),
         jnp.zeros((seq_count, token_count, head_count, HEAD_DIM), jnp.float32),
     )
-    key_shard = lax.all_gather(key_proj, "sp", axis=1, tiled=True)
+    ring = [key_proj]
+    for hop in range(3):
+        ring.append(lax.ppermute(ring[-1], "sp", [(dev, (dev + 1) % 4) for dev in range(4)]))
+    key_shard = jnp.roll(
+        jnp.concatenate(ring[::-1], axis=1), (lax.axis_index("sp") + 1) * ring[0].shape[1], axis=1
+    )
     value_shard = lax.all_gather(value_proj, "sp", axis=1, tiled=True)
     key_total = key_shard.shape[1]
     block_rows = 512

time: 484 us -> 427 us (0.88)
  waiting for transfers between devices: 374 us -> 298 us
  local copies, waits for them, and re-layouts: 27 us -> 40.8 us
  starting transfers between devices: 4.34 us -> 9.66 us
    all_gather x1 -> x0, waiting for transfers between devices: 75.1 us -> none  [on_device(): key_shard = lax.all_gather(key_proj, 'sp', axis=1, tiled=True)]
    ppermute x0 -> x3, waiting for transfers between devices: none -> 57.6 us  [on_device(): lax.ppermute(ring[-1], 'sp', [(dev, (dev + 1) % 4) for dev in range(4)])]
    all_gather x1, waiting for transfers between devices: 74.5 us -> 22.1 us  [on_device(): value_shard = lax.all_gather(value_proj, 'sp', axis=1, tiled=True)]
    unnamed x22 -> x35, local copies, waits for them, and re-layouts: 17 us -> 24.3 us
    ppermute x0 -> x3, starting transfers between devices: none -> 5.36 us  [on_device(): lax.ppermute(ring[-1], 'sp', [(dev, (dev + 1) % 4) for dev in range(4)])]
  transfers between devices with their start and end apart: 11 -> 13, of which waited for: 9 -> 9; matrix products, arithmetic and copies ran while one was open for 16% -> 21% of each run, Pallas kernels for 0% -> 0%
where the time goes in v1:
time: 427 us; the launch traced here: 426 us
  waiting for transfers between devices  298 us (70%)
  matrix products  46.3 us (11%)
  local copies, waits for them, and re-layouts  40.8 us (10%)
  other arithmetic  14.2 us (3%)
  between operations  13.6 us (3%)
  starting transfers between devices  9.66 us (2%)
    reduce_scatter x1, waiting for transfers between devices, on_device(): lax.psum_scatter((jnp.dot(pool_flat, out_pool_full, preferred_element_typ...  89.5 us
    all_gather x1, waiting for transfers between devices, on_device(): shard_rows = lax.all_gather(normed, 'tp', axis=1, tiled=True)  58.3 us
    ppermute x3, waiting for transfers between devices, on_device(): lax.ppermute(ring[-1], 'sp', [(dev, (dev + 1) % 4) for dev in range(4)])  57.6 us
    unnamed x35, local copies, waits for them, and re-layouts  24.3 us
    all_gather x1, waiting for transfers between devices, on_device(): value_shard = lax.all_gather(value_proj, 'sp', axis=1, tiled=True)  22.1 us
    all_gather x1, waiting for transfers between devices, on_device(): lax.all_gather(w_value, 'fs', axis=0, tiled=True)  19.9 us
    all_gather x1, waiting for transfers between devices, on_device(): lax.all_gather(w_key, 'fs', axis=0, tiled=True)  18.5 us
    all_gather x1, waiting for transfers between devices, on_device(): lax.all_gather(w_pool_in, 'fs', axis=0, tiled=True)  16.4 us
  transfers between devices with their start and end apart: 13, of which 9 were waited for; matrix products, arithmetic and copies ran while one was open for 21% of the time, Pallas kernels for 0%

profile of v1, /device:TPU:0, one launch (start us, length us, event | category | flops | bytes accessed | tf_op | source)
XLA Modules:
  0.0 425.9 jit_solution(2938594129094340023)
XLA Ops:
  14.4 19.9 %all-gather.19.cloned.1.call-done = bf16[2048,512]{1,0:T(8,128)(2,1)} async-done(((bf16[512,512]{1,0:T(8,128)(2,1)}), bf16[2048,512]{1,0:T(8,128)(2,1)}) %all-gather.19.cloned.1.call-update) | async-done | bytes 2097168 | tf_op jit(solution)/shard_map/all_gather | solution.py:83
  34.2 58.3 %all-gather.9.cloned.1.call-done = bf16[2,512,2048]{2,1,0:T(8,128)(2,1)} async-done(((bf16[2,256,2048]{2,1,0:T(8,128)(2,1)}), bf16[2,512,2048]{2,1,0:T(8,128)(2,1)}) %all-gather.9.cloned.1.call-update) | async-done | bytes 4194320 | tf_op jit(solution)/shard_map/all_gather | solution.py:89
  92.5 6.2 %fusion.35 = bf16[2,512,512]{2,1,0:T(8,128)(2,1)} fusion(bf16[2,512,2048]{2,1,0:T(8,128)(2,1)} %all-gather.9.cloned.1.call-done, bf16[2048,512]{1,0:T(8,128)(2,1)} %all-gather.19.cloned.1.call-done), kind=kOutput, calls=%fused_computation.44 | convolution fusion | flops 2148007936 | bytes 7340032 | tf_op jit(solution)/shard_map/dot_general | solution.py:97
  100.3 16.4 %all-gather.11.cloned.1.call-done = bf16[2048,512]{1,0:T(8,128)(2,1)} async-done(((bf16[512,512]{1,0:T(8,128)(2,1)}), bf16[2048,512]{1,0:T(8,128)(2,1)}) %all-gather.11.cloned.1.call-update) | async-done | bytes 2097168 | tf_op jit(solution)/shard_map/all_gather | solution.py:80
  116.7 5.2 %fusion.26 = bf16[2,512,512]{2,1,0:T(8,128)(2,1)S(1)} fusion(bf16[2,512,2048]{2,1,0:T(8,128)(2,1)} %all-gather.9.cloned.1.call-done, bf16[2048,512]{1,0:T(8,128)(2,1)} %all-gather.11.cloned.1.call-done), kind=kOutput, calls=%fused_computation.41 | convolution fusion | flops 2148007936 | bytes 7340032 | tf_op jit(solution)/shard_map/dot_general | solution.py:92
  122.2 18.5 %all-gather.15.cloned.1.call-done = bf16[2048,512]{1,0:T(8,128)(2,1)} async-done(((bf16[512,512]{1,0:T(8,128)(2,1)}), bf16[2048,512]{1,0:T(8,128)(2,1)}) %all-gather.15.cloned.1.call-update) | async-done | bytes 2097168 | tf_op jit(solution)/shard_map/all_gather | solution.py:82
  140.7 6.2 %fusion.29 = bf16[2,512,512]{2,1,0:T(8,128)(2,1)} fusion(bf16[2,512,2048]{2,1,0:T(8,128)(2,1)} %all-gather.9.cloned.1.call-done, bf16[2048,512]{1,0:T(8,128)(2,1)} %all-gather.15.cloned.1.call-done), kind=kOutput, calls=%fused_computation.42 | convolution fusion | flops 2148007936 | bytes 7340032 | tf_op jit(solution)/shard_map/dot_general | solution.py:96
  148.4 4.0 collective-permute-start
  152.4 12.3 %all-gather.17.cloned.1.call-done = bf16[2048,512]{0,1:T(8,128)(2,1)} async-done(((bf16[512,512]{0,1:T(8,128)(2,1)}), bf16[2048,512]{0,1:T(8,128)(2,1)}) %all-gather.17.cloned.1.call-update) | async-done | bytes 2097168 | tf_op jit(solution)/shard_map/all_gather | solution.py:81
  164.7 6.2 %fusion.32 = bf16[2,512,512]{1,2,0:T(8,128)(2,1)} fusion(bf16[2,512,2048]{2,1,0:T(8,128)(2,1)} %all-gather.9.cloned.1.call-done, bf16[2048,512]{0,1:T(8,128)(2,1)} %all-gather.17.cloned.1.call-done), kind=kOutput, calls=%fused_computation.43 | convolution fusion | flops 2148007936 | bytes 7340032 | tf_op jit(solution)/shard_map/dot_general | solution.py:93
  170.9 2.3 copy.39
  180.8 25.2 %collective-permute-done.2 = bf16[2,512,512]{2,1,0:T(8,128)(2,1)} collective-permute-done((bf16[2,512,512]{2,1,0:T(8,128)(2,1)}, bf16[2,512,512]{2,1,0:T(8,128)(2,1)}, u32[]{:S(2)}, u32[]{:S(2)}) %collective-permute-start.2) | collective-permute-done | bytes 1048608 | tf_op jit(solution)/shard_map/ppermute | solution.py:140
  216.4 7.3 %fusion.79 = f32[1024,2048]{1,0:T(8,128)} fusion(bf16[1024,512]{1,0:T(8,128)(2,1)S(1)} %bitcast.129, bf16[512,2048]{1,0:T(8,128)(2,1)} %all-gather.13.cloned.1.call-done), kind=kOutput, calls=%fused_computation.132 | convolution fusion | flops 2147483648 | bytes 11534336 | tf_op jit(solution)/shard_map/dot_general | solution.py:203
  223.7 32.4 %collective-permute-done.3 = bf16[2,512,512]{2,1,0:T(8,128)(2,1)S(1)} collective-permute-done((bf16[2,512,512]{2,1,0:T(8,128)(2,1)}, bf16[2,512,512]{2,1,0:T(8,128)(2,1)S(1)}, u32[]{:S(2)}, u32[]{:S(2)}) %collective-permute-start.3) | collective-permute-done | bytes 1048608 | tf_op jit(solution)/shard_map/ppermute | solution.py:140
  266.3 6.3 %copy.38 = bf16[2,2048,512]{1,2,0:T(8,128)(2,1)} copy(bf16[2,2048,512]{2,1,0:T(8,128)(2,1)} %constant_dynamic-slice_fusion.3) | data formatting | bytes 8388608
  272.6 22.1 %all-gather.21.cloned.1.call-done = bf16[2,2048,512]{2,1,0:T(8,128)(2,1)} async-done(((bf16[2,512,512]{2,1,0:T(8,128)(2,1)}), bf16[2,2048,512]{2,1,0:T(8,128)(2,1)}) %all-gather.21.cloned.1.call-update) | async-done | bytes 4194320 | tf_op jit(solution)/shard_map/all_gather | solution.py:144
  294.7 6.2 %copy.40 = bf16[2,2048,512]{1,2,0:T(8,128)(2,1)} copy(bf16[2,2048,512]{2,1,0:T(8,128)(2,1)} %all-gather.21.cloned.1.call-done) | data formatting | bytes 8388608
  302.2 17.2 %while.15 = (s32[]{:T(128)}, f32[2,512,4]{1,2,0:T(4,128)S(1)}, f32[2,512,4]{1,2,0:T(4,128)S(1)}, f32[2,512,4,128]{1,3,2,0:T(8,128)S(1)}, s32[4]{0:T(128)S(1)}, /...) while((s32[]{:T(128)}, f32[2,512,4]{1,2,0:T(4,128)S(1)}, ...), condition=%wide.region_6.7_spmd.clone, body=%wide.region_1.6_spmd.clone.sunk | while | flops 1114907648 | bytes 38154656 | solution.py:188
  303.5 12.0 %conditional.3 = ((f32[2,512,4]{1,2,0:T(4,128)S(1)}, f32[2,512,4]{1,2,0:T(4,128)S(1)}, f32[2,512,4,128]{1,3,2,0:T(8,128)S(1)})) conditional(s32[]{:T(128)} %convert_element_type.217, (f32[2,512,4]{1,2,0:T(4,128)S(1)}, f32[2,512,4]{1,2,0:T(4,128)S(1)}, f32[2,512,4,128]{1,3,2,0:T(8,128)S(1)}) %tuple.49, (s32[]{:T(128)}, s32[]{:T(128)}, s32[]{:T(128)}, ...), branch_computations={%region_2.2_spmd, %region_3.5_spmd} | conditional | flops 1114907648 | bytes 38152320 | solution.py:186
  306.1 2.6 fusion.6
  308.8 3.2 fusion.5
  312.0 3.5 bitcast_add_fusion.1
  321.5 8.4 %add_convert_fusion = bf16[1024,2048]{1,0:T(8,128)(2,1)} fusion(f32[1024,2048]{1,0:T(8,128)} %fusion.79, bf16[1024,512]{1,0:T(8,128)(2,1)S(1)} %bitcast.130, bf16[512,2048]{1,0:T(8,128)(2,1)} %all-gather.23.cloned.1.call-done), kind=kOutput, calls=%fused_computation.22 | convolution fusion | flops 2151677952 | bytes 15728640 | tf_op jit(solution)/shard_map/dot_general | solution.py:204
  329.9 89.5 %reduce-scatter.2.cloned.1.call-done = bf16[512,2048]{1,0:T(8,128)(2,1)} async-done(((bf16[1024,2048]{1,0:T(8,128)(2,1)}), bf16[512,2048]{1,0:T(8,128)(2,1)}) %reduce-scatter.2.cloned.1.call-update) | async-done | bytes 2097168 | tf_op jit(solution)/shard_map/reduce_scatter | solution.py:201
  (115 shorter events, 46.7 us)
Async XLA Ops:
  6.5 173.9 %copy-start = (bf16[8,128,128]{2,1,0:T(8,128)(2,1)S(1)}, bf16[8,128,128]{2,1,0:T(8,128)(2,1)}, u32[]{:S(2)}) copy-start(bf16[8,128,128]{2,1,0:T(8,128)(2,1)} %param.18) | copy-start | bytes 786436
  6.5 2.9 copy-start.4
  6.5 2.9 copy-start.9
  6.5 27.7 %all-gather.19.cloned.1.call-start = ((), (), s32[]{:S(2)}) async-start(), calls=%async_computation.6 | async-start | bytes 2621440 | tf_op jit(solution)/shard_map/all_gather | solution.py:83
  7.3 85.2 %all-gather.9.cloned.1.call-start = ((), (), s32[]{:S(2)}) async-start(), calls=%async_computation.1 | async-start | bytes 6291456 | tf_op jit(solution)/shard_map/all_gather | solution.py:89
  11.3 1.4 copy-start.7
  11.3 105.4 %all-gather.11.cloned.1.call-start = ((), (), s32[]{:S(2)}) async-start(), calls=%async_computation.2 | async-start | bytes 2621440 | tf_op jit(solution)/shard_map/all_gather | solution.py:80
  12.0 128.6 %all-gather.15.cloned.1.call-start = ((), (), s32[]{:S(2)}) async-start(), calls=%async_computation.4 | async-start | bytes 2621440 | tf_op jit(solution)/shard_map/all_gather | solution.py:82
  12.6 152.1 %all-gather.17.cloned.1.call-start = ((), (), s32[]{:S(2)}) async-start(), calls=%async_computation.5 | async-start | bytes 2621440 | tf_op jit(solution)/shard_map/all_gather | solution.py:81
  13.7 202.7 %all-gather.13.cloned.1.call-start = ((), (), s32[]{:S(2)}) async-start(), calls=%async_computation.3 | async-start | bytes 2621440 | tf_op jit(solution)/shard_map/all_gather | solution.py:84
  14.3 85.3 %copy-start.8 = (f32[2,4,2048]{2,1,0:T(4,128)S(1)}, f32[2,4,2048]{2,1,0:T(4,128)}, u32[]{:S(2)}) copy-start(f32[2,4,2048]{2,1,0:T(4,128)} %param.23) | copy-start | bytes 196612
  14.3 85.4 %copy-start.11 = (f32[1024]{0:T(1024)S(1)}, f32[1024]{0:T(1024)}, u32[]{:S(2)}) copy-start(f32[1024]{0:T(1024)} %param.19) | copy-start | bytes 12292
  14.3 280.4 %all-gather.21.cloned.1.call-start = ((), (), s32[]{:S(2)}) async-start(), calls=%async_computation.7 | async-start | bytes 5242880 | tf_op jit(solution)/shard_map/all_gather | solution.py:144
  98.7 222.7 %all-gather.23.cloned.1.call-start = ((), (), s32[]{:S(2)}) async-start(), calls=%async_computation.8 | async-start | bytes 2621440 | tf_op jit(solution)/shard_map/all_gather | solution.py:85
  99.5 319.9 %reduce-scatter.2.cloned.1.call-start = ((), (), s32[]{:S(2)}) async-start(), calls=%async_computation.9 | async-start | bytes 6291456 | tf_op jit(solution)/shard_map/reduce_scatter | solution.py:201
  146.9 29.7 %collective-permute-start.1 = (bf16[2,512,512]{2,1,0:T(8,128)(2,1)}, bf16[2,512,512]{2,1,0:T(8,128)(2,1)}, u32[]{:S(2)}, u32[]{:S(2)}) collective-permute-start(bf16[2,512,512]{2,1,0:T(8,128)(2,1)} %fusion.29), channel_id=1, source_target_pairs={{0,8},{8,16},{16,24},{24,0},{1,9},{9,17},{17,25},{25,1},{2,10},{10... | collective-permute-start | bytes 3145736 | tf_op jit(solution)/shard_map/ppermute | solution.py:140
  148.4 24.8 %collective-permute-start = (bf16[2,15,512]{2,1,0:T(8,128)(2,1)S(1)}, bf16[2,15,512]{2,1,0:T(8,128)(2,1)}, u32[]{:S(2)}, u32[]{:S(2)}) collective-permute-start(bf16[2,15,512]{2,1,0:T(8,128)(2,1)S(1)} %slice.84), channel_id=1, source_target_pairs={{0,8},{8,16},{16,24},{1,9},{9,17},{17,25},{2,10},{10,18},{18,26},{... | collective-permute-start | bytes 92168 | tf_op jit(solution)/shard_map/ppermute | solution.py:16
  176.3 2.0 copy-start.3
  176.3 2.0 slice-start
  176.6 29.5 %collective-permute-start.2 = (bf16[2,512,512]{2,1,0:T(8,128)(2,1)}, bf16[2,512,512]{2,1,0:T(8,128)(2,1)}, u32[]{:S(2)}, u32[]{:S(2)}) collective-permute-start(bf16[2,512,512]{2,1,0:T(8,128)(2,1)} %collective-permute-done.1), channel_id=1, source_target_pairs={{0,8},{8,16},{16,24},{24,0},{1,9},{9,17},{17,25},{25,1},{2,10},{10... | collective-permute-start | bytes 3145736 | tf_op jit(solution)/shard_map/ppermute | solution.py:140
  206.1 50.0 %collective-permute-start.3 = (bf16[2,512,512]{2,1,0:T(8,128)(2,1)}, bf16[2,512,512]{2,1,0:T(8,128)(2,1)S(1)}, u32[]{:S(2)}, u32[]{:S(2)}) collective-permute-start(bf16[2,512,512]{2,1,0:T(8,128)(2,1)} %collective-permute-done.2), channel_id=1, source_target_pairs={{0,8},{8,16},{16,24},{24,0},{1,9},{9,17},{17,25},{25,1},{2,10},{10... | collective-permute-start | bytes 3145736 | tf_op jit(solution)/shard_map/ppermute | solution.py:140
  212.5 2.3 copy-start.10
  213.2 1.6 copy-start.5
  329.9 89.5 %copy-start.1 = (bf16[8,128,128]{2,1,0:T(8,128)(2,1)S(1)}, bf16[8,128,128]{2,1,0:T(8,128)(2,1)}, u32[]{:S(2)}) copy-start(bf16[8,128,128]{2,1,0:T(8,128)(2,1)} %param.18) | copy-start | bytes 786436
  (2 other events, 2.3 us)
Sparse Core Ops, SparseCore 0:
  8.9 25.2 all-gather.18
  35.8 56.7 all-gather.8
  94.1 22.5 all-gather.10
  118.1 22.5 all-gather.14
  142.1 22.5 all-gather.16
  166.1 22.5 all-gather.12
  190.3 104.3 all-gather.20
  296.2 20.4 all-gather.22
  330.1 89.2 reduce-scatter.1
